TPU v7x, 32 devices: a whole 2x2x4 slice. The times are simulated.
32 devices in a mesh: sp: 16 (over z, y, core), tp: 2 (over x).
Axes of the slice: x: 2, y: 2, z: 4, core: 2. Of those that a mesh axis runs over, the one named last changes fastest.
Arguments:
- residual: bfloat16 [2048, 2048], P('sp', 'tp'), may hold values from -24 to 24
- queries: bfloat16 [2048, 2048], P('sp', 'tp'), may hold values from -16 to 16
- key_proj: bfloat16 [2048, 512], P(('sp', 'tp')), may hold values from -8 to 8
- value_proj: bfloat16 [2048, 512], P(('sp', 'tp')), may hold values from -6 to 6
- diff_lambda: float32 [8], replicated, may hold values from 0.3 to 0.8
- head_gain: float32 [256], replicated, may hold values from 0.1 to 1.9
- out_weight: bfloat16 [2048, 2048], P(None, 'tp'), may hold values from -0.125 to 0.125
- norm_gain: float32 [2048], P('tp'), may hold values from 0.1 to 1.9
- up_weight: bfloat16 [2048, 8192], P('sp', 'tp'), may hold values from -0.125 to 0.125
- down_weight: bfloat16 [8192, 2048], P('tp', 'sp'), may hold values from -0.0625 to 0.0625
Outputs:
- layer_out: bfloat16 [2048, 2048], P('sp', 'tp')
All inputs are finite; a program needn't handle non-finite values.
Results may differ from a plain program's by a relative error of at most 0.012.
Values may be sent and summed in bfloat16 or wider, within the bound.
A program may use at most 128 MiB of HBM per device.

v0:
```python
import jax
import jax.numpy as jnp
from jax import lax
from jax.sharding import PartitionSpec as P

D = 2048
HEADS = 8
KV_HEADS = 2
HEAD_DIM = 128
VALUE_DIM = 256


epsilon = 1e-06


def head_norm(per_map, lambdas, gain):
    difference = per_map[:, 0] - lambdas[:, None, None] * per_map[:, 1]
    scaled = (
        difference
        * lax.rsqrt(jnp.mean(difference * difference, axis=-1, keepdims=True) + epsilon)
        * gain
    )
    return scaled.astype(jnp.bfloat16)


def on_device(
    residual,
    queries,
    key_proj,
    value_proj,
    diff_lambda,
    head_gain,
    out_weight,
    norm_gain,
    up_weight,
    down_weight,
):
    rows_here = residual.shape[0]
    per_group = HEADS // KV_HEADS
    scaling = HEAD_DIM ** (-0.5)
    all_queries = lax.all_gather(queries, "tp", axis=1, tiled=True)
    query_grid = all_queries.reshape(rows_here, KV_HEADS, per_group, 2, HEAD_DIM)
    stat_shape = (KV_HEADS, per_group, 2, rows_here)
    maxima = jnp.full(stat_shape, -1e30, jnp.float32)
    key_piece = lax.all_gather(key_proj, "sp", axis=0, tiled=True)
    value_piece = lax.all_gather(value_proj, "sp", axis=0, tiled=True)
    key_count = key_piece.shape[0]
    key_grid = key_piece.reshape(key_count, KV_HEADS, 2, HEAD_DIM)
    value_grid = value_piece.reshape(key_count, KV_HEADS, VALUE_DIM)
    scores = (
        jnp.einsum("qagcd,kacd->agcqk", query_grid, key_grid, preferred_element_type=jnp.float32)
        * scaling
    )
    highest = jnp.maximum(maxima, jnp.max(scores, axis=-1))
    weights = jnp.exp(scores - highest[..., None])
    totals = jnp.sum(weights, axis=-1)
    weighted = jnp.einsum(
        "agcqk,kae->agcqe",
        weights.astype(jnp.bfloat16),
        value_grid,
        preferred_element_type=jnp.float32,
    )
    maxima, totals, weighted = (highest, totals, weighted)
    maxima = maxima.reshape(HEADS, 2, rows_here)
    totals = totals.reshape(HEADS, 2, rows_here)
    weighted = weighted.reshape(HEADS, 2, rows_here, VALUE_DIM)
    tp_size = lax.axis_size("tp")
    local_heads = HEADS // tp_size
    got_max, got_tot, got_sum = (
        lax.all_to_all(maxima, "tp", split_axis=0, concat_axis=0, tiled=True),
        lax.all_to_all(totals, "tp", split_axis=0, concat_axis=0, tiled=True),
        lax.all_to_all(weighted, "tp", split_axis=0, concat_axis=0, tiled=True),
    )
    got_max = got_max.reshape(tp_size, local_heads, 2, rows_here)
    got_tot = got_tot.reshape(tp_size, local_heads, 2, rows_here)
    got_sum = got_sum.reshape(tp_size, local_heads, 2, rows_here, VALUE_DIM)
    highest = jnp.max(got_max, axis=0)
    factor = jnp.exp(got_max - highest)
    totals_all = jnp.sum(factor * got_tot, axis=0)
    sums_all = jnp.sum(factor[..., None] * got_sum, axis=0)
    lambdas = lax.dynamic_slice_in_dim(diff_lambda, lax.axis_index("tp") * local_heads, local_heads)
    own_heads = head_norm(sums_all / totals_all[..., None], lambdas, head_gain)
    head_outputs = lax.all_gather(own_heads, "tp", axis=0, tiled=True)
    out_grid = out_weight.reshape(HEADS, VALUE_DIM, out_weight.shape[1])
    projected = jnp.einsum(
        "hqe,hed->qd", head_outputs, out_grid, preferred_element_type=jnp.float32
    )
    after_mix = residual.astype(jnp.float32) + projected
    squares = lax.psum(jnp.sum(after_mix * after_mix, axis=1), "tp")
    normed = (after_mix * lax.rsqrt(squares / D + epsilon)[:, None] * norm_gain).astype(
        jnp.bfloat16
    )
    full_rows = lax.all_gather(normed, "tp", axis=1, tiled=True)
    hidden = jnp.dot(
        full_rows,
        lax.all_gather(up_weight, "sp", axis=0, tiled=True),
        preferred_element_type=jnp.float32,
    )
    activated = jnp.square(jax.nn.relu(hidden)).astype(jnp.bfloat16)
    partial_value = jnp.dot(
        activated,
        lax.all_gather(down_weight, "sp", axis=1, tiled=True),
        preferred_element_type=jnp.float32,
    )
    mixer_sum = lax.psum_scatter(partial_value, "tp", scatter_dimension=1, tiled=True)
    return (after_mix + mixer_sum).astype(jnp.bfloat16)


def solution(mesh):
    return jax.shard_map(
        on_device,
        mesh=mesh,
        in_specs=(
            P("sp", "tp"),
            P("sp", "tp"),
            P(("sp", "tp"), None),
            P(("sp", "tp"), None),
            P(),
            P(),
            P(None, "tp"),
            P("tp"),
            P("sp", "tp"),
            P("tp", "sp"),
        ),
        out_specs=P("sp", "tp"),
        check_vma=False,
    )
```

profile of v0, /device:TPU:0, one launch (start us, length us, event | category | flops | bytes accessed | tf_op | source)
XLA Modules:
  0.0 390.0 jit_solution(11635504555220988634)
XLA Ops:
  6.5 0.0 all-gather.5.cloned.1.call-start
  6.5 0.7 all-gather.5.cloned.1.call-update
  7.3 0.0 all-gather.7.cloned.1.call-start
  7.3 0.7 all-gather.7.cloned.1.call-update
  8.0 0.0 all-gather.11.cloned.1.call-start
  8.1 0.7 all-gather.11.cloned.1.call-update
  8.7 0.0 all-gather.9.cloned.1.call-start
  8.8 0.5 all-gather.9.cloned.1.call-update
  9.3 1.1 copy.32
  10.4 9.9 %all_gather.22 = bf16[128,2048]{0,1:T(8,128)(2,1)S(1)} all-gather(bf16[128,1024]{0,1:T(8,128)(2,1)S(1)} %copy.32), channel_id=1, replica_groups=mesh['sp'=16,'tp'=2] {'tp'}, dimensions={1}, use_global_device_ids=true | all-gather | bytes 786432 | tf_op jit(solution)/shard_map/all_gather | solution.py:41
  20.4 29.7 %all-gather.5.cloned.1.call-done = bf16[1024,512]{1,0:T(8,128)(2,1)} async-done(((bf16[64,512]{1,0:T(8,128)(2,1)}), bf16[1024,512]{1,0:T(8,128)(2,1)}) %all-gather.5.cloned.1.call-update) | async-done | bytes 1048592 | tf_op jit(solution)/shard_map/all_gather | solution.py:45
  50.1 1.5 copy.31
  51.6 4.5 %bitcast_reduce_fusion = (f32[2,4,2,128]{3,1,2,0:T(4,128)S(1)}, f32[2,2,1024,128,4]{3,2,4,1,0:T(8,128)}) fusion(bf16[1024,2,2,128,1]{0,3,4,2,1:T(8,128)(2,1)S(1)} %bitcast.61, bf16[128,2,4,2,128]{0,4,3,2,1:T(8,128)(2,1)S(1)} %bitcast.62), kind=kOutput, calls=%fused_computation.1 | convolution fusion | flops 541063168 | bytes 9969664 | tf_op jit(solution)/shard_map/qagcd,kacd->agcqk/dot_general | solution.py:51
  56.1 0.6 copy.36
  56.7 3.2 all-to-all-start
  60.0 5.6 %fusion.1 = (f32[2,4,2,128]{3,1,2,0:T(4,128)S(1)}, bf16[2,4,2,128,1024]{3,4,1,2,0:T(8,128)(2,1)}) fusion(f32[2,2,1024,128,4]{3,2,4,1,0:T(8,128)} %get-tuple-element.8, f32[2,4,2,128]{3,1,2,0:T(4,128)S(1)} %broadcast_maximum_fusion), kind=kLoop, calls=%fused_computation.3 | loop fusion | flops 8386560 | bytes 12599296 | tf_op jit(solution)/shard_map/reduce_sum | solution.py:56
  65.6 0.6 copy.41
  66.2 23.0 %all-gather.7.cloned.1.call-done = bf16[1024,512]{1,0:T(8,128)(2,1)} async-done(((bf16[64,512]{1,0:T(8,128)(2,1)}), bf16[1024,512]{1,0:T(8,128)(2,1)}) %all-gather.7.cloned.1.call-update) | async-done | bytes 1048592 | tf_op jit(solution)/shard_map/all_gather | solution.py:46
  89.1 1.5 copy.37
  90.6 0.0 all-to-all-done
  90.6 3.2 all-to-all-start.2
  93.9 0.0 copy-start.4
  93.9 5.2 %fusion.5 = f32[2,4,2,128,256]{4,3,2,1,0:T(8,128)} fusion(bf16[1024,2,256,1,1]{0,2,4,3,1:T(8,128)(2,1)S(1)} %bitcast.64, bf16[2,4,2,128,1024]{3,4,1,2,0:T(8,128)(2,1)} %get-tuple-element.6), kind=kOutput, calls=%fused_computation.8 | convolution fusion | flops 1073741824 | bytes 7340032 | tf_op jit(solution)/shard_map/agcqk,kae->agcqe/dot_general | solution.py:57
  99.1 0.0 all-to-all-done.2
  99.1 3.8 all-to-all-start.1
  102.9 0.0 copy-start.3
  103.0 0.0 reduce-scatter.2.cloned.1.call-start
  103.0 0.0 copy-done.4
  103.0 0.1 dynamic_slice.3
  103.2 25.3 %all-to-all-done.1 = f32[8,2,128,256]{3,2,1,0:T(8,128)S(1)} async-done(((f32[8,2,128,256]{3,2,1,0:T(8,128)}), f32[8,2,128,256]{3,2,1,0:T(8,128)S(1)}, u32[]{:S(2)}, u32[]{:S(2)}) %all-to-all-start.1) | async-done | bytes 2097184 | tf_op jit(solution)/shard_map/all_to_all | solution.py:72
  128.4 0.3 multiply_reduce_fusion
  128.8 0.2 broadcast_divide_fusion
  129.0 0.0 copy-start.2
  129.0 0.2 multiply_reduce_fusion.2
  129.2 0.0 copy-done.3
  129.2 0.1 multiply_convert_fusion.1
  129.4 8.5 %all_gather.24 = bf16[8,128,256]{2,1,0:T(8,128)(2,1)S(1)} all-gather(bf16[4,128,256]{2,1,0:T(8,128)(2,1)S(1)} %multiply_convert_fusion.1), channel_id=1, replica_groups=mesh['sp'=16,'tp'=2] {'tp'}, dimensions={0}, use_global_device_ids=true | all-gather | bytes 786432 | tf_op jit(solution)/shard_map/all_gather | solution.py:83
  137.9 0.0 copy-done
  137.9 0.8 multiply_reduce_fusion.1
  138.7 4.9 %psum.7 = f32[128]{0:T(128)S(1)} all-reduce(f32[128]{0:T(128)S(1)} %get-tuple-element.9), channel_id=1, replica_groups=mesh['sp'=16,'tp'=2] {'tp'}, use_global_device_ids=true, to_apply=%region_7.0 | all-reduce | flops 128 | bytes 1024 | tf_op jit(solution)/shard_map/psum | solution.py:89
  143.6 0.1 multiply_convert_fusion
  143.8 7.0 %all_gather.25 = bf16[128,2048]{1,0:T(8,128)(2,1)S(1)} all-gather(bf16[128,1024]{1,0:T(8,128)(2,1)S(1)} %multiply_convert_fusion), channel_id=1, replica_groups=mesh['sp'=16,'tp'=2] {'tp'}, dimensions={1}, use_global_device_ids=true | all-gather | bytes 786432 | tf_op jit(solution)/shard_map/all_gather | solution.py:93
  150.8 69.3 %all-gather.11.cloned.1.call-done = bf16[4096,2048]{1,0:T(8,128)(2,1)} async-done(((bf16[4096,128]{1,0:T(8,128)(2,1)}), bf16[4096,2048]{1,0:T(8,128)(2,1)}) %all-gather.11.cloned.1.call-update) | async-done | bytes 16777232 | tf_op jit(solution)/shard_map/all_gather | solution.py:102
  220.1 126.7 %all-gather.9.cloned.1.call-done = bf16[2048,4096]{1,0:T(8,128)(2,1)} async-done(((bf16[128,4096]{1,0:T(8,128)(2,1)}), bf16[2048,4096]{1,0:T(8,128)(2,1)}) %all-gather.9.cloned.1.call-update) | async-done | bytes 16777232 | tf_op jit(solution)/shard_map/all_gather | solution.py:96
  346.9 16.1 %fusion.8 = f32[128,2048]{1,0:T(8,128)} fusion(bf16[4096,2048]{1,0:T(8,128)(2,1)} %all-gather.11.cloned.1.call-done, bf16[128,2048]{1,0:T(8,128)(2,1)S(1)} %all_gather.25, bf16[2048,4096]{1,0:T(8,128)(2,1)} %all-gather.9.cloned.1.call-done), kind=kOutput, calls=%fused_computation.13 | convolution fusion | flops 4296540160 | bytes 35127296 | tf_op jit(solution)/shard_map/dot_general | solution.py:100
  362.9 0.0 reduce-scatter.2.cloned.1.call-update
  362.9 18.7 %reduce-scatter.2.cloned.1.call-done = f32[128,1024]{1,0:T(8,128)} async-done(((f32[128,2048]{1,0:T(8,128)}), f32[128,1024]{1,0:T(8,128)}) %reduce-scatter.2.cloned.1.call-update) | async-done | bytes 524304 | tf_op jit(solution)/shard_map/reduce_scatter | solution.py:105
  381.7 1.8 add_convert_fusion
  (12 shorter events, 0.1 us)
Async XLA Ops:
  6.5 43.6 %all-gather.5.cloned.1.call-start = ((), (), s32[]{:S(2)}) async-start(), calls=%async_computation.4 | async-start | bytes 1114112 | tf_op jit(solution)/shard_map/all_gather | solution.py:45
  7.3 81.9 %all-gather.7.cloned.1.call-start = ((), (), s32[]{:S(2)}) async-start(), calls=%async_computation.5 | async-start | bytes 1114112 | tf_op jit(solution)/shard_map/all_gather | solution.py:46
  8.0 212.1 %all-gather.11.cloned.1.call-start = ((), (), s32[]{:S(2)}) async-start(), calls=%async_computation.7 | async-start | bytes 17825792 | tf_op jit(solution)/shard_map/all_gather | solution.py:102
  8.7 338.1 %all-gather.9.cloned.1.call-start = ((), (), s32[]{:S(2)}) async-start(), calls=%async_computation.6 | async-start | bytes 17825792 | tf_op jit(solution)/shard_map/all_gather | solution.py:96
  56.7 33.9 %all-to-all-start = ((f32[8,2,128]{2,1,0:T(2,128)}), f32[8,2,128]{2,1,0:T(2,128)S(1)}, u32[]{:S(2)}, u32[]{:S(2)}) async-start(f32[8,2,128]{2,1,0:T(2,128)} %copy.36), calls=%async_computation | async-start | bytes 16384 | tf_op jit(solution)/shard_map/all_to_all | solution.py:70
  90.6 8.5 %all-to-all-start.2 = ((f32[8,2,128]{2,1,0:T(2,128)}), f32[8,2,128]{2,1,0:T(2,128)S(1)}, u32[]{:S(2)}, u32[]{:S(2)}) async-start(f32[8,2,128]{2,1,0:T(2,128)} %copy.41), calls=%async_computation.2 | async-start | bytes 16384 | tf_op jit(solution)/shard_map/all_to_all | solution.py:71
  93.9 9.1 %copy-start.4 = (f32[8]{0:T(128)S(1)}, f32[8]{0:T(128)}, u32[]{:S(2)}) copy-start(f32[8]{0:T(128)} %param.14) | copy-start | bytes 100
  99.1 29.3 %all-to-all-start.1 = ((f32[8,2,128,256]{3,2,1,0:T(8,128)}), f32[8,2,128,256]{3,2,1,0:T(8,128)S(1)}, u32[]{:S(2)}, u32[]{:S(2)}) async-start(f32[8,2,128,256]{3,2,1,0:T(8,128)} %bitcast.63), calls=%async_computation.1 | async-start | bytes 4194304 | tf_op jit(solution)/shard_map/all_to_all | solution.py:72
  102.9 26.3 %copy-start.3 = (f32[256]{0:T(256)S(1)}, f32[256]{0:T(256)}, u32[]{:S(2)}) copy-start(f32[256]{0:T(256)} %param.15) | copy-start | bytes 3076
  103.0 278.7 %reduce-scatter.2.cloned.1.call-start = ((), (), s32[]{:S(2)}) async-start(), calls=%async_computation.8 | async-start | bytes 1572864 | tf_op jit(solution)/shard_map/reduce_scatter | solution.py:105
  128.4 9.4 %copy-start = (bf16[2048,1024]{1,0:T(8,128)(2,1)S(1)}, bf16[2048,1024]{1,0:T(8,128)(2,1)}, u32[]{:S(2)}) copy-start(bf16[2048,1024]{1,0:T(8,128)(2,1)} %param.16) | copy-start | bytes 12582916
  128.4 9.4 %copy-start.1 = (bf16[128,1024]{1,0:T(8,128)(2,1)S(1)}, bf16[128,1024]{1,0:T(8,128)(2,1)}, u32[]{:S(2)}) copy-start(bf16[128,1024]{1,0:T(8,128)(2,1)} %param.10) | copy-start | bytes 786436
  129.0 14.7 %copy-start.2 = (f32[1024]{0:T(1024)S(1)}, f32[1024]{0:T(1024)}, u32[]{:S(2)}) copy-start(f32[1024]{0:T(1024)} %param.17) | copy-start | bytes 12292
Sparse Core Ops, SparseCore 0:
  9.5 40.5 all-gather.4
  52.3 36.8 all-gather.6
  91.3 128.7 all-gather.10
  222.2 124.6 all-gather.8
  363.1 18.5 reduce-scatter.1
where the time goes:
time: 390 us
  waiting for transfers between devices  295 us (76%)
  blocking collectives  30.4 us (8%)
  matrix products  26.6 us (7%)
  between operations  13.3 us (3%)
  starting transfers between devices  10.4 us (3%)
  other arithmetic  8.51 us (2%)
  local copies, waits for them, and re-layouts  5.4 us (1%)
    all_gather x1, waiting for transfers between devices, on_device(): lax.all_gather(up_weight, 'sp', axis=0, tiled=True)  127 us
    all_gather x1, waiting for transfers between devices, on_device(): lax.all_gather(down_weight, 'sp', axis=1, tiled=True)  69.3 us
    all_gather x1, waiting for transfers between devices, on_device(): key_piece = lax.all_gather(key_proj, 'sp', axis=0, tiled=True)  29.7 us
    all_to_all x1, waiting for transfers between devices, on_device(): lax.all_to_all(weighted, 'tp', split_axis=0, concat_axis=0, tiled=True)  25.3 us
    all_gather x1, waiting for transfers between devices, on_device(): value_piece = lax.all_gather(value_proj, 'sp', axis=0, tiled=True)  23 us
    reduce_scatter x1, waiting for transfers between devices, on_device(): lax.psum_scatter(partial_value, 'tp', scatter_dimension=1, tiled=True)  18.7 us
    dot_general x1, matrix products, on_device(): jnp.dot(activated, lax.all_gather(down_weight, 'sp', axis=1, tiled=True),...  16.1 us
    all_gather x1, blocking collectives, on_device(): all_queries = lax.all_gather(queries, 'tp', axis=1, tiled=True)  9.94 us
  transfers between devices with their start and end apart: 8, of which 6 were waited for; matrix products, arithmetic and copies ran while one was open for 6% of the time, Pallas kernels for 0%

commit v1 on v0

--- a/solution.py
+++ b/solution.py
@@ -1,6 +1,11 @@
+import functools
+import math
+
 import jax
 import jax.numpy as jnp
 from jax import lax
+from jax.experimental import pallas as pl
+from jax.experimental.pallas import tpu as pltpu
 from jax.sharding import PartitionSpec as P
 
 D = 2048
@@ -106,9 +111,297 @@
     return (after_mix + mixer_sum).astype(jnp.bfloat16)
 
 
+MESH = pl.DeviceIdType.MESH
+F32 = jnp.float32
+BF16 = jnp.bfloat16
+CHIP_CORES = 2
+Y_CHIPS = 2
+
+
+def fused_kernel(
+    layers, residual, queries, keys, values, lambdas, head_gain, out_weight, norm_gain,
+    up, down, out,
+    kv_all, up_all, down_all, q_buf, res_buf, w_buf, heads_all, squares, tokens,
+    part_out, part_in, sum_out, sum_in, after, own_part, local_sem, send_sem, recv_sem,
+):
+    x = lax.axis_index("tp")
+    s = lax.axis_index("sp")
+    core, y, z = s % CHIP_CORES, (s // CHIP_CORES) % Y_CHIPS, s // (CHIP_CORES * Y_CHIPS)
+
+    def place(z_, y_, c_):
+        return (z_ * Y_CHIPS + y_) * CHIP_CORES + c_
+
+    def z_back(d):
+        return lax.rem(z - d + layers, layers)
+
+    def z_ahead(d):
+        return lax.rem(z + d, layers)
+
+    mate = {"sp": s, "tp": 1 - x}
+    beside = {"sp": place(z, 1 - y, core), "tp": x}
+    twin = {"sp": place(z, y, 1 - core), "tp": x}
+    column = [{"sp": place(z_ahead(d), y, core), "tp": x} for d in range(layers)]
+
+    barrier = pltpu.get_barrier_semaphore()
+    peers = [mate, beside, twin] + column[1:]
+    for peer in peers:
+        pl.semaphore_signal(barrier, inc=1, device_id=peer, device_id_type=MESH)
+
+    count = {"local": 0, "remote": 0}
+    started = []
+
+    def bring(src, dst):
+        copy = pltpu.make_async_copy(src, dst, local_sem.at[count["local"]])
+        count["local"] += 1
+        copy.start()
+        return copy
+
+    def send(src, dst, peer):
+        i = count["remote"]
+        count["remote"] += 1
+        copy = pltpu.make_async_remote_copy(
+            src_ref=src, dst_ref=dst, send_sem=send_sem.at[i], recv_sem=recv_sem.at[i],
+            device_id=peer, device_id_type=MESH,
+        )
+        copy.start()
+        started.append(copy)
+        return copy
+
+    few = keys.shape[0]
+    kw = kv_all.shape[2] // 2
+    chunk = up_all.shape[2]
+    lanes = down.shape[1]
+
+    def half(ref, part):
+        return ref.at[:, pl.ds(pl.multiple_of(part * kw, kw), kw)]
+
+    def kv_rows(block, part, side):
+        return kv_all.at[block, pl.ds(pl.multiple_of(part * few, few), few), pl.ds(side * kw, kw)]
+
+    own_kv = [bring(half(keys, x), kv_rows(s, x, 0)), bring(half(values, x), kv_rows(s, x, 1))]
+    q_copy = bring(queries, q_buf)
+
+    pl.semaphore_wait(barrier, len(peers))
+
+    swapped = [
+        send(half(keys, 1 - x), kv_rows(s, x, 0), mate),
+        send(half(values, 1 - x), kv_rows(s, x, 1), mate),
+    ]
+    for copy in own_kv:
+        copy.wait()
+    for copy in swapped:
+        copy.wait_recv()
+    kv_z = [None] + [send(kv_all.at[s], kv_all.at[s], column[d]) for d in range(1, layers)]
+
+    def up_chunk(part):
+        return up.at[:, pl.ds(pl.multiple_of(part * chunk, chunk), chunk)]
+
+    def down_chunk(part):
+        return down.at[pl.ds(pl.multiple_of(part * chunk, chunk), chunk), :]
+
+    def up_block(b):
+        return up_all.at[b]
+
+    def down_block(b):
+        return down_all.at[:, pl.ds(pl.multiple_of(b * lanes, lanes), lanes)]
+
+    up_z = [None] + [send(up_chunk(z_ahead(d)), up_block(s), column[d]) for d in range(1, layers)]
+    up_own = bring(up_chunk(z), up_block(s))
+    down_own = bring(down_chunk(z), down_block(s))
+    w_copy = bring(out_weight, w_buf)
+    r_copy = bring(residual, res_buf)
+
+    def spread(block_of, d, arrival):
+        if arrival is not None:
+            arrival()
+        b = block_of(place(z_back(d), y, core))
+        return send(b, b, beside), send(b, b, twin)
+
+    def pass_on(block_of, d, came):
+        came.wait_recv()
+        b = block_of(place(z_back(d), 1 - y, core))
+        return send(b, b, twin)
+
+    def kv_block(b):
+        return kv_all.at[b]
+
+    kv_y, kv_t, kv_u = [], [], []
+    for d in range(layers):
+        to_y, to_t = spread(kv_block, d, kv_z[d].wait_recv if d else None)
+        kv_y.append(to_y)
+        kv_t.append(to_t)
+        if d:
+            kv_u.append(pass_on(kv_block, d - 1, kv_y[d - 1]))
+    kv_u.append(pass_on(kv_block, layers - 1, kv_y[layers - 1]))
+
+    up_y, up_t, up_u = {}, {}, {}
+    down_y, down_t, down_u = {}, {}, {}
+    up_y[0], up_t[0] = spread(up_block, 0, up_own.wait)
+    down_z = [None] + [
+        send(down_chunk(z_ahead(d)), down_block(s), column[d]) for d in range(1, layers)
+    ]
+    for copy in kv_t + kv_u:
+        copy.wait_recv()
+    q_copy.wait()
+
+    local_heads = q_buf.shape[1] // (2 * HEAD_DIM)
+    blocks, per_block = kv_all.shape[0], kv_all.shape[1]
+    key_count = blocks * per_block
+    factor = HEAD_DIM ** (-0.5) * math.log2(math.e)
+    vals = lambda: kv_all[:, :, kw:].reshape(key_count, kw)
+    head_copies = []
+    for h in range(local_heads):
+        maps = []
+        for c in range(2):
+            q = q_buf[:, (2 * h + c) * HEAD_DIM : (2 * h + c + 1) * HEAD_DIM]
+            k = kv_all[:, :, c * HEAD_DIM : (c + 1) * HEAD_DIM].reshape(key_count, HEAD_DIM)
+            scores = lax.dot_general(q, k, (((1,), (1,)), ((), ())), preferred_element_type=F32)
+            top = jnp.max(scores, axis=1, keepdims=True)
+            weights = jnp.exp2((scores - top) * factor)
+            total = jnp.sum(weights, axis=1, keepdims=True)
+            summed = jnp.dot(weights.astype(BF16), vals(), preferred_element_type=F32)
+            maps.append(summed / total)
+        diff = maps[0] - lambdas[x * local_heads + h] * maps[1]
+        scaled = diff * lax.rsqrt(jnp.mean(diff * diff, axis=1, keepdims=True) + epsilon)
+        where = heads_all.at[x, :, pl.ds(h * VALUE_DIM, VALUE_DIM)]
+        heads_all[x, :, pl.ds(h * VALUE_DIM, VALUE_DIM)] = (scaled * head_gain[...]).astype(BF16)
+        head_copies.append(send(where, where, mate))
+        if 1 <= h < layers:
+            up_y[h], up_t[h] = spread(up_block, h, up_z[h].wait_recv)
+            up_u[h - 1] = pass_on(up_block, h - 1, up_y[h - 1])
+    for d in range(max(local_heads, 1), layers):
+        up_y[d], up_t[d] = spread(up_block, d, up_z[d].wait_recv)
+        up_u[d - 1] = pass_on(up_block, d - 1, up_y[d - 1])
+
+    wide = heads_all.shape[2]
+    w_copy.wait()
+    r_copy.wait()
+
+    def w_rows(part):
+        return w_buf[pl.ds(pl.multiple_of(part * wide, wide), wide), :]
+
+    mix = res_buf[...].astype(F32) + jnp.dot(heads_all[x], w_rows(x), preferred_element_type=F32)
+    down_y[0], down_t[0] = spread(down_block, 0, down_own.wait)
+    for copy in head_copies:
+        copy.wait_recv()
+    mix = mix + jnp.dot(heads_all[1 - x], w_rows(1 - x), preferred_element_type=F32)
+    after[...] = mix
+    own_squares = jnp.sum(mix * mix, axis=1, keepdims=True)
+    squares[x] = jnp.broadcast_to(own_squares, squares.shape[1:])
+    sq_copy = send(squares.at[x], squares.at[x], mate)
+    up_u[layers - 1] = pass_on(up_block, layers - 1, up_y[layers - 1])
+    sq_copy.wait_recv()
+    width = 2 * wide
+    mean = (own_squares + squares[1 - x][:, :1]) / width
+    tokens[z, x] = (after[...] * lax.rsqrt(mean + epsilon) * norm_gain[...]).astype(BF16)
+
+    mine = tokens.at[z, x]
+    tok_z = [None] + [send(mine, mine, column[d]) for d in range(1, layers)]
+    tok_x = [send(mine, mine, mate)]
+    for d in range(1, layers):
+        down_y[d], down_t[d] = spread(down_block, d, down_z[d].wait_recv)
+        down_u[d - 1] = pass_on(down_block, d - 1, down_y[d - 1])
+    down_u[layers - 1] = pass_on(down_block, layers - 1, down_y[layers - 1])
+    for d in range(1, layers):
+        tok_z[d].wait_recv()
+        block = tokens.at[z_back(d), x]
+        tok_x.append(send(block, block, mate))
+    for group in (up_t, up_u, down_t, down_u):
+        for d in range(layers):
+            group[d].wait_recv()
+
+    up_half = up_all.shape[0] // 2
+    order = list(range(layers))
+    part_copies, sum_copies = {}, {}
+
+    def up_rows(i):
+        return up_all[i * up_half : (i + 1) * up_half].reshape(wide, chunk)
+
+    def settle(d):
+        part_copies[d].wait_recv()
+        both = own_part[d] + part_in[d].astype(F32)
+        if d == 0:
+            after[...] = after[...] + both
+        else:
+            sum_out[d - 1] = both.astype(BF16)
+            back = {"sp": place(z_back(d), y, core), "tp": x}
+            sum_copies[d] = send(sum_out.at[d - 1], sum_in.at[d - 1], back)
+
+    for i, d in enumerate(order):
+        zb = z_back(d)
+        tok_x[d].wait_recv()
+        hidden = jnp.dot(tokens[zb, 0], up_rows(0), preferred_element_type=F32) + jnp.dot(
+            tokens[zb, 1], up_rows(1), preferred_element_type=F32
+        )
+        activated = jnp.square(jnp.maximum(hidden, 0.0)).astype(BF16)
+
+        def down_cols(part):
+            return down_all[:, pl.ds(pl.multiple_of(part * wide, wide), wide)]
+
+        part_out[d] = jnp.dot(activated, down_cols(1 - x), preferred_element_type=F32).astype(BF16)
+        part_copies[d] = send(part_out.at[d], part_in.at[d], mate)
+        own_part[d] = jnp.dot(activated, down_cols(x), preferred_element_type=F32)
+        if i:
+            settle(order[i - 1])
+    settle(order[-1])
+    result = after[...]
+    for d in range(1, layers):
+        sum_copies[d].wait_recv()
+        result = result + sum_in[d - 1].astype(F32)
+    out[...] = result.astype(out.dtype)
+    for copy in started:
+        copy.wait_send()
+
+
+def on_chip(sp_size, residual, queries, key_proj, value_proj, diff_lambda, head_gain, out_weight,
+            norm_gain, up_weight, down_weight):
+    layers = sp_size // (CHIP_CORES * Y_CHIPS)
+    rows, wide = residual.shape
+    kw = key_proj.shape[1] // KV_HEADS
+    chunk = up_weight.shape[1] // layers
+    hbm = pl.BlockSpec(memory_space=pltpu.HBM)
+    vmem = pl.BlockSpec(memory_space=pltpu.VMEM)
+    smem = pl.BlockSpec(memory_space=pltpu.SMEM)
+    copies = 2 + 3 * (layers - 1) + 3 * 3 * layers + wide // VALUE_DIM + 1 + 3 * layers + layers
+    return pl.pallas_call(
+        functools.partial(fused_kernel, layers),
+        out_shape=jax.ShapeDtypeStruct(residual.shape, BF16),
+        in_specs=[hbm, hbm, hbm, hbm, smem, vmem, hbm, vmem, hbm, hbm],
+        out_specs=vmem,
+        scratch_shapes=[
+            pltpu.VMEM((sp_size, 2 * key_proj.shape[0], 2 * kw), BF16),
+            pltpu.VMEM((sp_size, up_weight.shape[0], chunk), BF16),
+            pltpu.VMEM((chunk, sp_size * down_weight.shape[1]), BF16),
+            pltpu.VMEM(queries.shape, BF16),
+            pltpu.VMEM(residual.shape, BF16),
+            pltpu.VMEM(out_weight.shape, BF16),
+            pltpu.VMEM((2, rows, wide), BF16),
+            pltpu.VMEM((2, rows, 128), F32),
+            pltpu.VMEM((layers, 2, rows, wide), BF16),
+            pltpu.VMEM((layers, rows, wide), BF16),
+            pltpu.VMEM((layers, rows, wide), BF16),
+            pltpu.VMEM((layers - 1, rows, wide), BF16),
+            pltpu.VMEM((layers - 1, rows, wide), BF16),
+            pltpu.VMEM((rows, wide), F32),
+            pltpu.VMEM((layers, rows, wide), F32),
+            pltpu.SemaphoreType.DMA((8,)),
+            pltpu.SemaphoreType.DMA((copies,)),
+            pltpu.SemaphoreType.DMA((copies,)),
+        ],
+        compiler_params=pltpu.CompilerParams(
+            collective_id=0, has_side_effects=True, vmem_limit_bytes=60 * 2**20
+        ),
+        name="fused_layer",
+    )(residual, queries, key_proj, value_proj, diff_lambda, head_gain.reshape(1, -1), out_weight,
+      norm_gain.reshape(1, -1), up_weight, down_weight)
+
+
 def solution(mesh):
+    sp_size, tp_size = mesh.shape["sp"], mesh.shape["tp"]
+    direct = tp_size == KV_HEADS == 2 and sp_size % (CHIP_CORES * Y_CHIPS) == 0
+    body = functools.partial(on_chip, sp_size) if direct else on_device
     return jax.shard_map(
-        on_device,
+        body,
         mesh=mesh,
         in_specs=(
             P("sp", "tp"),

time: 390 us -> 140 us (0.36)
  waiting for transfers between devices: 295 us -> 0 us
  Pallas kernels: 0 us -> 137 us
  blocking collectives: 30.4 us -> 0 us
  matrix products: 26.6 us -> 0 us
  between operations: 13.3 us -> 0.01 us
  starting transfers between devices: 10.4 us -> 0 us
  other arithmetic: 8.51 us -> 0 us
    all_gather x4 -> x0, waiting for transfers between devices: 249 us -> none  [the longest x1 127 us: on_device(): lax.all_gather(up_weight, 'sp', axis=0, tiled=True)]
    pallas_call x0 -> x1, Pallas kernels: none -> 137 us  [on_chip(): pl.pallas_call(functools.partial(fused_kernel, layers), out_shape=jax.Sha...]
    dot_general x4 -> x0, matrix products: 26.6 us -> none  [the longest x1 16.1 us: on_device(): jnp.dot(activated, lax.all_gather(down_weight, 'sp', axis=1, tiled=True),...]
    all_gather x3 -> x0, blocking collectives: 25.5 us -> none  [the longest x1 9.94 us: on_device(): all_queries = lax.all_gather(queries, 'tp', axis=1, tiled=True)]
    all_to_all x3 -> x0, waiting for transfers between devices: 25.3 us -> none  [the longest x1 25.3 us: on_device(): lax.all_to_all(weighted, 'tp', split_axis=0, concat_axis=0, tiled=True)]
    reduce_scatter x1 -> x0, waiting for transfers between devices: 18.7 us -> none  [on_device(): lax.psum_scatter(partial_value, 'tp', scatter_dimension=1, tiled=True)]
    all_to_all x3 -> x0, starting transfers between devices: 10.3 us -> none  [the longest x1 3.8 us: on_device(): lax.all_to_all(weighted, 'tp', split_axis=0, concat_axis=0, tiled=True)]
    reduce_sum x4 -> x0, other arithmetic: 6.19 us -> none  [the longest x1 5.62 us: on_device(): totals = jnp.sum(weights, axis=-1)]
  transfers between devices with their start and end apart: 8 -> 0, of which waited for: 6 -> 0; matrix products, arithmetic and copies ran while one was open for 6% -> 0% of each run, Pallas kernels for 0% -> 0%
where the time goes in v1:
time: 140 us; the launch traced here: 138 us
  Pallas kernels  137 us (98%)
  local copies, waits for them, and re-layouts  1.67 us (1%)
    pallas_call x1, Pallas kernels, on_chip(): pl.pallas_call(functools.partial(fused_kernel, layers), out_shape=jax.Sha...  137 us

profile of v1, /device:TPU:0, one launch (start us, length us, event | category | flops | bytes accessed | tf_op | source)
XLA Modules:
  0.0 138.4 jit_solution(18251830234042560655)
XLA Ops:
  0.0 136.7 %fused_layer.1 = bf16[128,1024]{1,0:T(8,128)(2,1)} custom-call(bf16[128,1024]{1,0:T(8,128)(2,1)} %residual.1, bf16[128,1024]{1,0:T(8,128)(2,1)} %queries.1, bf16[64,512]{1,0:T(8,128)(2,1)} %keys.1, bf16[64,512]{1,0:T(8,128)(2,1)} %values.1, f32[8]{0:T(128)} %lambdas.1, f32[1,256]{1,0:T(1,128)} %bitcast.3, bf16[2048,1024]{1,0:T(8,128)(2,1)} %out_weight.1, ...), custom_call_target="tpu_custom_call" | custom-call | tf_op jit(solution)/shard_map/fused_layer/pallas_call | solution.py:366
  136.7 1.7 %copy.12 = bf16[128,1024]{1,0:T(8,128)(2,1)} copy(bf16[128,1024]{1,0:T(8,128)(2,1)} %fused_layer.1) | data formatting | bytes 524288

commit v2 on v1

--- a/solution.py
+++ b/solution.py
@@ -225,6 +225,8 @@
     def kv_block(b):
         return kv_all.at[b]
 
+    up_y, up_t, up_u = {}, {}, {}
+    down_y, down_t, down_u = {}, {}, {}
     kv_y, kv_t, kv_u = [], [], []
     for d in range(layers):
         to_y, to_t = spread(kv_block, d, kv_z[d].wait_recv if d else None)
@@ -232,14 +234,14 @@
         kv_t.append(to_t)
         if d:
             kv_u.append(pass_on(kv_block, d - 1, kv_y[d - 1]))
+        else:
+            up_y[0], up_t[0] = spread(up_block, 0, up_own.wait)
+            down_z = [None] + [
+                send(down_chunk(z_ahead(e)), down_block(s), column[e]) for e in range(1, layers)
+            ]
     kv_u.append(pass_on(kv_block, layers - 1, kv_y[layers - 1]))
 
-    up_y, up_t, up_u = {}, {}, {}
-    down_y, down_t, down_u = {}, {}, {}
-    up_y[0], up_t[0] = spread(up_block, 0, up_own.wait)
-    down_z = [None] + [
-        send(down_chunk(z_ahead(d)), down_block(s), column[d]) for d in range(1, layers)
-    ]
+    down_y[0], down_t[0] = spread(down_block, 0, down_own.wait)
     for copy in kv_t + kv_u:
         copy.wait_recv()
     q_copy.wait()
@@ -268,10 +270,8 @@
         head_copies.append(send(where, where, mate))
         if 1 <= h < layers:
             up_y[h], up_t[h] = spread(up_block, h, up_z[h].wait_recv)
-            up_u[h - 1] = pass_on(up_block, h - 1, up_y[h - 1])
     for d in range(max(local_heads, 1), layers):
         up_y[d], up_t[d] = spread(up_block, d, up_z[d].wait_recv)
-        up_u[d - 1] = pass_on(up_block, d - 1, up_y[d - 1])
 
     wide = heads_all.shape[2]
     w_copy.wait()
@@ -281,7 +281,6 @@
         return w_buf[pl.ds(pl.multiple_of(part * wide, wide), wide), :]
 
     mix = res_buf[...].astype(F32) + jnp.dot(heads_all[x], w_rows(x), preferred_element_type=F32)
-    down_y[0], down_t[0] = spread(down_block, 0, down_own.wait)
     for copy in head_copies:
         copy.wait_recv()
     mix = mix + jnp.dot(heads_all[1 - x], w_rows(1 - x), preferred_element_type=F32)
@@ -289,7 +288,6 @@
     own_squares = jnp.sum(mix * mix, axis=1, keepdims=True)
     squares[x] = jnp.broadcast_to(own_squares, squares.shape[1:])
     sq_copy = send(squares.at[x], squares.at[x], mate)
-    up_u[layers - 1] = pass_on(up_block, layers - 1, up_y[layers - 1])
     sq_copy.wait_recv()
     width = 2 * wide
     mean = (own_squares + squares[1 - x][:, :1]) / width
@@ -297,21 +295,30 @@
 
     mine = tokens.at[z, x]
     tok_z = [None] + [send(mine, mine, column[d]) for d in range(1, layers)]
-    tok_x = [send(mine, mine, mate)]
+    tok_x = {0: send(mine, mine, mate)}
     for d in range(1, layers):
+        up_u[d - 1] = pass_on(up_block, d - 1, up_y[d - 1])
         down_y[d], down_t[d] = spread(down_block, d, down_z[d].wait_recv)
-        down_u[d - 1] = pass_on(down_block, d - 1, down_y[d - 1])
-    down_u[layers - 1] = pass_on(down_block, layers - 1, down_y[layers - 1])
-    for d in range(1, layers):
+    up_u[layers - 1] = pass_on(up_block, layers - 1, up_y[layers - 1])
+    down_u[0] = pass_on(down_block, 0, down_y[0])
+
+    def cross(d):
         tok_z[d].wait_recv()
         block = tokens.at[z_back(d), x]
-        tok_x.append(send(block, block, mate))
+        tok_x[d] = send(block, block, mate)
+
+    order = list(range(1, layers)) + [0]
+    for d in order[:1]:
+        cross(d)
+    for d in range(1, layers):
+        down_u[d] = pass_on(down_block, d, down_y[d])
+    for d in order[1:-1][:1]:
+        cross(d)
     for group in (up_t, up_u, down_t, down_u):
         for d in range(layers):
             group[d].wait_recv()
 
     up_half = up_all.shape[0] // 2
-    order = list(range(layers))
     part_copies, sum_copies = {}, {}
 
     def up_rows(i):
@@ -341,6 +348,8 @@
         part_out[d] = jnp.dot(activated, down_cols(1 - x), preferred_element_type=F32).astype(BF16)
         part_copies[d] = send(part_out.at[d], part_in.at[d], mate)
         own_part[d] = jnp.dot(activated, down_cols(x), preferred_element_type=F32)
+        if i + 2 < layers - 1:
+            cross(order[i + 2])
         if i:
             settle(order[i - 1])
     settle(order[-1])

time: 140 us -> 132 us (0.943)
  Pallas kernels: 137 us -> 130 us
    pallas_call x1, Pallas kernels: 137 us -> 130 us  [on_chip(): pl.pallas_call(functools.partial(fused_kernel, layers), out_shape=jax.Sha...]
where the time goes in v2:
time: 132 us; the launch traced here: 131 us
  Pallas kernels  130 us (98%)
  local copies, waits for them, and re-layouts  1.67 us (1%)
    pallas_call x1, Pallas kernels, on_chip(): pl.pallas_call(functools.partial(fused_kernel, layers), out_shape=jax.Sha...  130 us

profile of v2, /device:TPU:0, one launch (start us, length us, event | category | flops | bytes accessed | tf_op | source)
XLA Modules:
  0.0 131.5 jit_solution(11076652639723622613)
XLA Ops:
  0.0 129.8 %fused_layer.1 = bf16[128,1024]{1,0:T(8,128)(2,1)} custom-call(bf16[128,1024]{1,0:T(8,128)(2,1)} %residual.1, bf16[128,1024]{1,0:T(8,128)(2,1)} %queries.1, bf16[64,512]{1,0:T(8,128)(2,1)} %keys.1, bf16[64,512]{1,0:T(8,128)(2,1)} %values.1, f32[8]{0:T(128)} %lambdas.1, f32[1,256]{1,0:T(1,128)} %bitcast.3, bf16[2048,1024]{1,0:T(8,128)(2,1)} %out_weight.1, ...), custom_call_target="tpu_custom_call" | custom-call | tf_op jit(solution)/shard_map/fused_layer/pallas_call | solution.py:375
  129.8 1.7 %copy.12 = bf16[128,1024]{1,0:T(8,128)(2,1)} copy(bf16[128,1024]{1,0:T(8,128)(2,1)} %fused_layer.1) | data formatting | bytes 524288
